TPU v7x, 512 devices: a 8x2x16 block of a 8x16x16 slice. The times are simulated.
512 devices in a mesh: grp: 2 (over y), tp: 16 (over z), dp: 16 (over x, core).
Axes of the slice: x: 8, y: 2, z: 16, core: 2. Of those that a mesh axis runs over, the one named last changes fastest.
The devices are a block of a 8x16x16 slice.
Arguments:
- tokens: bfloat16 [256, 4096], P(('grp', 'tp'), 'dp'), parts along dimension 0, may hold values from -50 to 50
- norm_gain: float32 [2, 4096], P(None, 'dp'), may hold values from 0.1 to 1.9
- query_weight: bfloat16 [2, 4096, 4096], P(None, 'dp', 'tp'), may hold values from -0.09375 to 0.09375
- key_weight: bfloat16 [2, 4096, 4096], P(None, 'dp', 'tp'), may hold values from -0.09375 to 0.09375
- value_weight: bfloat16 [2, 4096, 4096], P(None, 'dp', 'tp'), may hold values from -0.09375 to 0.09375
- outgate_weight: bfloat16 [2, 4096, 4096], P(None, 'dp', 'tp'), may hold values from -0.09375 to 0.09375
- input_gate_weight: bfloat16 [2, 4096, 64], P(None, 'dp', 'tp'), may hold values from -0.09375 to 0.09375
- forget_gate_weight: bfloat16 [2, 4096, 64], P(None, 'dp', 'tp'), may hold values from -0.09375 to 0.09375
- forget_bias: float32 [2, 64], P(None, 'tp'), may hold values from -2 to 5
- out_weight: bfloat16 [2, 4096, 4096], P(None, 'tp', 'dp'), may hold values from -0.09375 to 0.09375
- memory_state: float32 [2, 256, 64, 4096], P(None, ('grp', 'dp'), 'tp'), parts along dimension 1, may hold values from -0.9 to 0.9
- normalizer_state: float32 [2, 256, 4096], P(None, ('grp', 'dp'), 'tp'), parts along dimension 1, may hold values from -0.9 to 0.9
- maximum_state: float32 [2, 256, 64], P(None, ('grp', 'dp'), 'tp'), parts along dimension 1, may hold values from -1 to 1
Outputs:
- next_tokens: bfloat16 [256, 4096], P(('grp', 'tp'), 'dp'), parts along dimension 0
- next_memory: float32 [2, 256, 64, 4096], P(None, ('grp', 'dp'), 'tp'), parts along dimension 1
- next_normalizer: float32 [2, 256, 4096], P(None, ('grp', 'dp'), 'tp'), parts along dimension 1
- next_maximum: float32 [2, 256, 64], P(None, ('grp', 'dp'), 'tp'), parts along dimension 1
There are 2 independent parts, one for each index of `grp`. A program takes and returns all parts, laid end to end along the dimension named above; an argument that names none is the same for every part. Nothing has to cross between parts.
All inputs are finite; a program needn't handle non-finite values.
Results may differ from a plain program's by a relative error of at most 0.0074.
Values may be sent and summed in bfloat16 or wider, within the bound.
A program may use at most 64 MiB of HBM per device.

v0:
```python
import jax
import jax.numpy as jnp
from jax import lax
from jax.sharding import PartitionSpec as P

D = 4096
HEAD = 64


EPS = 1e-06


def from_everyone(array, axis):
    copies = jnp.broadcast_to(array, (lax.axis_size(axis), *array.shape))
    return lax.all_to_all(copies, axis, split_axis=0, concat_axis=0, tiled=True)


def laid_out(tiles, dim):
    tiles = jnp.moveaxis(tiles, 0, dim)
    lengths = tiles.shape
    return tiles.reshape(*lengths[:dim], lengths[dim] * lengths[dim + 1], *lengths[dim + 2 :])


def gather_directly(array, axis, dim):
    tiles = from_everyone(array, axis)
    return laid_out(tiles, dim)


def split_up(array, dim, size):
    before, after = (array.shape[:dim], array.shape[dim + 1 :])
    return jnp.moveaxis(array.reshape(*before, size, -1, *after), dim, 0)


def sent_and_summed(array, axis, dim):
    tiles = split_up(array, dim, lax.axis_size(axis))
    arrived = lax.all_to_all(tiles, axis, split_axis=0, concat_axis=0, tiled=True)
    return arrived.sum(axis=0)


def in_one_piece(arrays, axis, dim, along):
    columns = [a.reshape(*a.shape[:along], -1) for a in arrays]
    both = jnp.concatenate(columns, axis=along)
    whole, at, gathered = (sent_and_summed(both, axis, dim), 0, [])
    for a, column in zip(arrays, columns):
        piece = whole[..., at : at + column.shape[along]]
        gathered.append(piece.reshape(*piece.shape[:along], *a.shape[along:]))
        at += column.shape[along]
    return tuple(gathered)


def gather_rows(token_rows):
    return gather_directly(token_rows, "tp", 0)


def head_sum_rows(partial_value):
    return sent_and_summed(partial_value, "tp", 0)


def cell_layer(
    x_all,
    layer_idx,
    norm_gain,
    query_weight,
    key_weight,
    value_weight,
    outgate_weight,
    input_gate_weight,
    forget_gate_weight,
    forget_bias,
    out_weight,
    memory_state,
    normalizer_state,
    maximum_state,
):
    x_float = x_all.astype(jnp.float32)
    squares = jnp.sum(x_float * x_float, axis=1)
    scaled = (x_float * norm_gain[layer_idx][None, :]).astype(jnp.bfloat16)
    joined = jnp.concatenate(
        [
            query_weight[layer_idx],
            key_weight[layer_idx],
            value_weight[layer_idx],
            outgate_weight[layer_idx],
        ],
        axis=1,
    )
    gate_joined = jnp.concatenate(
        [input_gate_weight[layer_idx], forget_gate_weight[layer_idx]], axis=1
    )
    products = jnp.dot(scaled, joined, preferred_element_type=jnp.float32)
    gate_terms = jnp.dot(scaled, gate_joined, preferred_element_type=jnp.float32)
    products, gate_terms, squares = in_one_piece((products, gate_terms, squares), "dp", 0, 1)
    inv_rms = lax.rsqrt(squares / D + EPS)[:, None]
    width = query_weight.shape[2]
    head_count = width // HEAD
    row_count = products.shape[0]
    stored = lax.optimization_barrier((inv_rms * products).astype(jnp.bfloat16)).astype(jnp.float32)
    shape = (row_count, head_count, HEAD)
    query_vec = stored[:, 0:width].reshape(shape)
    key_vec = stored[:, width : 2 * width].reshape(shape) * HEAD ** (-0.5)
    value_vec = stored[:, 2 * width : 3 * width].reshape(shape)
    gate_vec = stored[:, 3 * width : 4 * width].reshape(shape)
    gate_pre = inv_rms * gate_terms
    input_pre = gate_pre[:, 0:head_count]
    forget_pre = gate_pre[:, head_count : 2 * head_count] + forget_bias[layer_idx][None, :]
    log_forget = jax.nn.log_sigmoid(forget_pre)
    old_max = maximum_state[layer_idx]
    new_max = jnp.maximum(log_forget + old_max, input_pre)
    keep_rate = jnp.exp(log_forget + old_max - new_max)
    admit_rate = jnp.exp(input_pre - new_max)
    memory = memory_state[layer_idx].reshape(row_count, head_count, HEAD, HEAD)
    memory = (
        keep_rate[:, :, None, None] * memory
        + admit_rate[:, :, None, None] * key_vec[:, :, :, None] * value_vec[:, :, None, :]
    )
    normalizer = (
        keep_rate[:, :, None] * normalizer_state[layer_idx].reshape(shape)
        + admit_rate[:, :, None] * key_vec
    )
    numerator = jnp.einsum("bhd,bhde->bhe", query_vec, memory, precision=lax.Precision.HIGHEST)
    denominator = jnp.sum(query_vec * normalizer, axis=2)
    readout = numerator / jnp.maximum(jnp.abs(denominator), jnp.exp(-new_max))[:, :, None]
    mixed = (readout * jax.nn.sigmoid(gate_vec)).astype(jnp.bfloat16).reshape(row_count, width)
    projection = out_weight[layer_idx]
    partial_value = jnp.dot(
        gather_directly(mixed, "dp", 0), projection, preferred_element_type=jnp.float32
    )
    return (
        partial_value,
        memory.reshape(row_count, head_count, HEAD * HEAD),
        normalizer.reshape(row_count, width),
        new_max,
    )


def per_device(
    tokens,
    norm_gain,
    query_weight,
    key_weight,
    value_weight,
    outgate_weight,
    input_gate_weight,
    forget_gate_weight,
    forget_bias,
    out_weight,
    memory_state,
    normalizer_state,
    maximum_state,
):
    weights = (
        norm_gain,
        query_weight,
        key_weight,
        value_weight,
        outgate_weight,
        input_gate_weight,
        forget_gate_weight,
        forget_bias,
        out_weight,
        memory_state,
        normalizer_state,
        maximum_state,
    )
    x_first = gather_rows(tokens)
    partial_value, memory_first, normalizer_first, maximum_first = cell_layer(x_first, 0, *weights)
    own_rows = (tokens.astype(jnp.float32) + head_sum_rows(partial_value)).astype(jnp.bfloat16)
    x_second = gather_rows(own_rows)
    partial_value, memory_second, normalizer_second, maximum_second = cell_layer(
        x_second, 1, *weights
    )
    next_tokens = (own_rows.astype(jnp.float32) + head_sum_rows(partial_value)).astype(jnp.bfloat16)
    return (
        next_tokens,
        jnp.stack([memory_first, memory_second]),
        jnp.stack([normalizer_first, normalizer_second]),
        jnp.stack([maximum_first, maximum_second]),
    )


def solution(mesh):
    in_specs = (
        P(("grp", "tp"), "dp"),
        P(None, "dp"),
        P(None, "dp", "tp"),
        P(None, "dp", "tp"),
        P(None, "dp", "tp"),
        P(None, "dp", "tp"),
        P(None, "dp", "tp"),
        P(None, "dp", "tp"),
        P(None, "tp"),
        P(None, "tp", "dp"),
        P(None, ("grp", "dp"), "tp", None),
        P(None, ("grp", "dp"), "tp"),
        P(None, ("grp", "dp"), "tp"),
    )
    out_specs = (
        P(("grp", "tp"), "dp"),
        P(None, ("grp", "dp"), "tp", None),
        P(None, ("grp", "dp"), "tp"),
        P(None, ("grp", "dp"), "tp"),
    )
    return jax.shard_map(
        per_device, mesh=mesh, in_specs=in_specs, out_specs=out_specs, check_vma=False
    )
```

profile of v0, /device:TPU:80, one launch (start us, length us, event | category | flops | bytes accessed | tf_op | source)
XLA Modules:
  0.0 198.4 jit_solution(11745802936802900671)
XLA Ops:
  0.6 1.3 broadcast_in_dim.8
  2.0 43.7 %all-to-all-start = ((bf16[16,8,256]{2,1,0:T(8,128)(2,1)}), bf16[16,8,256]{2,1,0:T(8,128)(2,1)S(1)}, u32[]{:S(2)}, u32[]{:S(2)}) async-start(bf16[16,8,256]{2,1,0:T(8,128)(2,1)} %broadcast_in_dim.8), calls=%async_computation | async-start | bytes 131072 | tf_op jit(solution)/shard_map/all_to_all | solution.py:15
  45.7 1.2 slice_bitcast_fusion.4
  46.9 0.7 copy-done.13
  47.6 10.7 %all-to-all-done = bf16[16,8,256]{2,1,0:T(8,128)(2,1)S(1)} async-done(((bf16[16,8,256]{2,1,0:T(8,128)(2,1)}), bf16[16,8,256]{2,1,0:T(8,128)(2,1)S(1)}, u32[]{:S(2)}, u32[]{:S(2)}) %all-to-all-start) | async-done | bytes 65568 | tf_op jit(solution)/shard_map/all_to_all | solution.py:15
  58.3 0.1 fusion.23
  58.4 0.2 copy.41
  58.6 0.1 fusion.35
  58.7 0.3 fusion.6
  59.0 0.9 concatenate.27
  59.9 7.6 %all-to-all-start.1 = ((f32[16,8,1033]{2,1,0:T(8,128)}), f32[16,8,1033]{2,1,0:T(8,128)S(1)}, u32[]{:S(2)}, u32[]{:S(2)}) async-start(f32[16,8,1033]{2,1,0:T(8,128)} %concatenate.27), calls=%async_computation.1 | async-start | bytes 1179648 | tf_op jit(solution)/shard_map/all_to_all | solution.py:36
  67.5 1.0 slice-done
  68.6 0.5 reshape_squeeze.12
  69.1 0.2 copy-done.10
  69.3 0.7 slice-done.3
  70.1 0.6 copy-done.14
  70.7 13.7 %all-to-all-done.1 = f32[16,8,1033]{2,1,0:T(8,128)S(1)} async-done(((f32[16,8,1033]{2,1,0:T(8,128)}), f32[16,8,1033]{2,1,0:T(8,128)S(1)}, u32[]{:S(2)}, u32[]{:S(2)}) %all-to-all-start.1) | async-done | bytes 528928 | tf_op jit(solution)/shard_map/all_to_all | solution.py:36
  84.5 0.2 fusion.57
  84.8 0.5 copy-done.6
  85.4 0.6 slice-done.1
  86.1 0.1 exponential_multiply_fusion.1
  86.2 0.1 subtract_exponential_fusion.1
  86.6 0.2 multiply_reduce_fusion.1
  86.8 0.8 fusion.3
  87.7 12.1 %all_to_all.40 = bf16[16,8,256]{2,1,0:T(8,128)(2,1)S(1)} all-to-all(bf16[16,8,256]{2,1,0:T(8,128)(2,1)S(1)} %broadcast_in_dim.9), channel_id=1, replica_groups=mesh['grp'=2,'tp'=16,'dp'=16] {'dp'}, dimensions={0} | all-to-all | bytes 131072 | tf_op jit(solution)/shard_map/all_to_all | solution.py:15
  99.8 0.2 fusion.28
  100.0 16.4 %all_to_all.41 = f32[16,8,256]{2,1,0:T(8,128)S(1)} all-to-all(f32[16,8,256]{2,1,0:T(8,128)S(1)} %fusion.28), channel_id=1, replica_groups=mesh['grp'=2,'tp'=16,'dp'=16] {'tp'}, dimensions={0} | all-to-all | bytes 262144 | tf_op jit(solution)/shard_map/all_to_all | solution.py:36
  116.4 0.7 copy-done.9
  117.1 18.3 %all_to_all.42 = bf16[16,8,256]{2,1,0:T(8,128)(2,1)S(1)} all-to-all(bf16[16,8,256]{2,1,0:T(8,128)(2,1)S(1)} %broadcast_in_dim.10), channel_id=1, replica_groups=mesh['grp'=2,'tp'=16,'dp'=16] {'tp'}, dimensions={0} | all-to-all | bytes 131072 | tf_op jit(solution)/shard_map/all_to_all | solution.py:15
  135.4 0.1 fusion.25
  135.5 0.2 copy.44
  135.7 0.1 fusion.32
  135.8 0.3 fusion.13
  136.1 0.9 concatenate.31
  137.0 4.0 %all-to-all-start.5 = ((f32[16,8,1033]{2,1,0:T(8,128)}), f32[16,8,1033]{2,1,0:T(8,128)S(1)}, u32[]{:S(2)}, u32[]{:S(2)}) async-start(f32[16,8,1033]{2,1,0:T(8,128)} %concatenate.31), calls=%async_computation.5 | async-start | bytes 1179648 | tf_op jit(solution)/shard_map/all_to_all | solution.py:36
  141.1 0.3 broadcast_multiply_fusion.1
  141.4 0.4 mul.289
  142.1 0.1 mul.293
  142.2 15.5 %all-to-all-done.5 = f32[16,8,1033]{2,1,0:T(8,128)S(1)} async-done(((f32[16,8,1033]{2,1,0:T(8,128)}), f32[16,8,1033]{2,1,0:T(8,128)S(1)}, u32[]{:S(2)}, u32[]{:S(2)}) %all-to-all-start.5) | async-done | bytes 528928 | tf_op jit(solution)/shard_map/all_to_all | solution.py:36
  157.7 0.2 fusion.54
  158.0 0.6 copy-done.7
  158.8 0.6 slice-done.2
  159.6 0.1 exponential_multiply_fusion
  159.8 0.1 mul.300
  159.9 0.1 subtract_exponential_fusion
  160.1 0.1 mul.298
  160.2 0.6 copy-done.8
  161.0 0.2 multiply_reduce_fusion
  161.1 0.3 broadcast_multiply_fusion
  161.5 0.4 mul.292
  161.9 0.8 copy-done
  162.7 1.4 multiply_add_fusion.1
  164.1 1.6 reshape_squeeze.14
  165.6 0.8 fusion
  166.6 0.6 broadcast_in_dim.11
  167.2 4.7 %all-to-all-start.6 = ((bf16[16,8,256]{2,1,0:T(8,128)(2,1)}), bf16[16,8,256]{2,1,0:T(8,128)(2,1)S(1)}, u32[]{:S(2)}, u32[]{:S(2)}) async-start(bf16[16,8,256]{2,1,0:T(8,128)(2,1)} %broadcast_in_dim.11), calls=%async_computation.6 | async-start | bytes 131072 | tf_op jit(solution)/shard_map/all_to_all | solution.py:15
  172.1 0.6 pad_maximum_fusion.1
  172.7 6.9 %all-to-all-done.6 = bf16[16,8,256]{2,1,0:T(8,128)(2,1)S(1)} async-done(((bf16[16,8,256]{2,1,0:T(8,128)(2,1)}), bf16[16,8,256]{2,1,0:T(8,128)(2,1)S(1)}, u32[]{:S(2)}, u32[]{:S(2)}) %all-to-all-start.6) | async-done | bytes 65568 | tf_op jit(solution)/shard_map/all_to_all | solution.py:15
  179.6 0.8 fusion.26
  180.4 4.0 %all-to-all-start.7 = ((f32[16,8,256]{2,1,0:T(8,128)}), f32[16,8,256]{2,1,0:T(8,128)S(1)}, u32[]{:S(2)}, u32[]{:S(2)}) async-start(f32[16,8,256]{2,1,0:T(8,128)} %fusion.26), calls=%async_computation.7 | async-start | bytes 262144 | tf_op jit(solution)/shard_map/all_to_all | solution.py:36
  184.4 0.6 pad_maximum_fusion.2
  185.0 1.2 pad_maximum_fusion
  186.2 11.6 %all-to-all-done.7 = f32[16,8,256]{2,1,0:T(8,128)S(1)} async-done(((f32[16,8,256]{2,1,0:T(8,128)}), f32[16,8,256]{2,1,0:T(8,128)S(1)}, u32[]{:S(2)}, u32[]{:S(2)}) %all-to-all-start.7) | async-done | bytes 131104 | tf_op jit(solution)/shard_map/all_to_all | solution.py:36
  197.8 0.6 add_convert_fusion
  (76 shorter events, 2.6 us)
Async XLA Ops:
  2.0 56.4 %all-to-all-start = ((bf16[16,8,256]{2,1,0:T(8,128)(2,1)}), bf16[16,8,256]{2,1,0:T(8,128)(2,1)S(1)}, u32[]{:S(2)}, u32[]{:S(2)}) async-start(bf16[16,8,256]{2,1,0:T(8,128)(2,1)} %broadcast_in_dim.8), calls=%async_computation | async-start | bytes 131072 | tf_op jit(solution)/shard_map/all_to_all | solution.py:15
  45.6 1.2 copy-start.11
  45.7 1.2 copy-start.12
  45.7 1.9 copy-start.4
  45.7 1.9 copy-start.5
  46.9 0.7 copy-start.13
  59.9 24.5 %all-to-all-start.1 = ((f32[16,8,1033]{2,1,0:T(8,128)}), f32[16,8,1033]{2,1,0:T(8,128)S(1)}, u32[]{:S(2)}, u32[]{:S(2)}) async-start(f32[16,8,1033]{2,1,0:T(8,128)} %concatenate.27), calls=%async_computation.1 | async-start | bytes 1179648 | tf_op jit(solution)/shard_map/all_to_all | solution.py:36
  67.5 1.0 slice-start
  68.5 0.7 copy-start.10
  69.3 0.7 slice-start.3
  70.0 0.7 copy-start.14
  84.7 0.6 copy-start.6
  85.3 0.7 slice-start.1
  86.7 13.0 %copy-start.3 = (bf16[2,256,256]{2,1,0:T(8,128)(2,1)S(1)}, bf16[2,256,256]{2,1,0:T(8,128)(2,1)}, u32[]{:S(2)}) copy-start(bf16[2,256,256]{2,1,0:T(8,128)(2,1)} %param.22) | copy-start | bytes 786436
  116.4 0.7 copy-start.9
  137.0 20.7 %all-to-all-start.5 = ((f32[16,8,1033]{2,1,0:T(8,128)}), f32[16,8,1033]{2,1,0:T(8,128)S(1)}, u32[]{:S(2)}, u32[]{:S(2)}) async-start(f32[16,8,1033]{2,1,0:T(8,128)} %concatenate.31), calls=%async_computation.5 | async-start | bytes 1179648 | tf_op jit(solution)/shard_map/all_to_all | solution.py:36
  158.0 0.6 copy-start.7
  158.7 0.7 slice-start.2
  160.1 0.7 copy-start.8
  161.5 1.2 copy-start
  165.6 19.3 %copy-start.2 = (f32[1,8,4,4096]{3,2,1,0:T(4,128)S(1)}, f32[1,8,4,4096]{3,2,1,0:T(4,128)}, u32[]{:S(2)}) copy-start(f32[1,8,4,4096]{3,2,1,0:T(4,128)} %get-tuple-element.17) | copy-start | bytes 1572868
  166.4 18.5 %copy-start.1 = (f32[1,8,4,4096]{3,2,1,0:T(4,128)S(1)}, f32[1,8,4,4096]{3,2,1,0:T(4,128)}, u32[]{:S(2)}) copy-start(f32[1,8,4,4096]{3,2,1,0:T(4,128)} %get-tuple-element.16) | copy-start | bytes 1572868
  167.2 12.3 %all-to-all-start.6 = ((bf16[16,8,256]{2,1,0:T(8,128)(2,1)}), bf16[16,8,256]{2,1,0:T(8,128)(2,1)S(1)}, u32[]{:S(2)}, u32[]{:S(2)}) async-start(bf16[16,8,256]{2,1,0:T(8,128)(2,1)} %broadcast_in_dim.11), calls=%async_computation.6 | async-start | bytes 131072 | tf_op jit(solution)/shard_map/all_to_all | solution.py:15
  180.4 17.4 %all-to-all-start.7 = ((f32[16,8,256]{2,1,0:T(8,128)}), f32[16,8,256]{2,1,0:T(8,128)S(1)}, u32[]{:S(2)}, u32[]{:S(2)}) async-start(f32[16,8,256]{2,1,0:T(8,128)} %fusion.26), calls=%async_computation.7 | async-start | bytes 262144 | tf_op jit(solution)/shard_map/all_to_all | solution.py:36
where the time goes:
time: 199 us; the launch traced here: 198 us
  starting transfers between devices  64 us (32%)
  waiting for transfers between devices  58.4 us (29%)
  blocking collectives  46.8 us (24%)
  local copies, waits for them, and re-layouts  18 us (9%)
  other arithmetic  6.93 us (3%)
  matrix products  3.3 us (2%)
    all_to_all x2, starting transfers between devices, from_everyone(): return lax.all_to_all(copies, axis, split_axis=0, concat_axis=0, tiled=True)  48.4 us
    all_to_all x3, waiting for transfers between devices, sent_and_summed(): lax.all_to_all(tiles, axis, split_axis=0, concat_axis=0, tiled=True)  40.9 us
    all_to_all x2, blocking collectives, from_everyone(): return lax.all_to_all(copies, axis, split_axis=0, concat_axis=0, tiled=True)  30.4 us
    all_to_all x2, waiting for transfers between devices, from_everyone(): return lax.all_to_all(copies, axis, split_axis=0, concat_axis=0, tiled=True)  17.5 us
    all_to_all x1, blocking collectives, sent_and_summed(): lax.all_to_all(tiles, axis, split_axis=0, concat_axis=0, tiled=True)  16.4 us
    all_to_all x3, starting transfers between devices, sent_and_summed(): lax.all_to_all(tiles, axis, split_axis=0, concat_axis=0, tiled=True)  15.6 us
    unnamed x30, local copies, waits for them, and re-layouts  4.68 us
  transfers between devices with their start and end apart: 5, of which 5 were waited for; matrix products, arithmetic and copies ran while one was open for 3% of the time, Pallas kernels for 0%

commit v1 on v0

v1 whole, which is shorter than its diff:
```python
import functools

import jax
import jax.numpy as jnp
from jax import lax
from jax.experimental import pallas as pl
from jax.experimental.pallas import tpu as pltpu
from jax.sharding import PartitionSpec as P

HEAD = 64
EPS = 1e-06
BATCH = 4
MESH = pl.DeviceIdType.MESH
F32 = jnp.float32
BF16 = jnp.bfloat16


def dot(a, b):
    return lax.dot_general(a, b, (((1,), (0,)), ((), ())), preferred_element_type=F32)


def lane_iota(shape):
    return lax.broadcasted_iota(jnp.int32, shape, 1)


def kernel(
    n,
    layers,
    tok_h,
    gain_h,
    qw_h,
    kw_h,
    vw_h,
    ow_h,
    ig_h,
    fg_h,
    fb_h,
    pw_h,
    mem_h,
    nrm_h,
    mx_h,
    tok_o,
    mem_o,
    nrm_o,
    mx_o,
    gain,
    w,
    gate_in,
    gate_w,
    fb,
    pw,
    mem,
    mem_t,
    nrm,
    mx,
    old_max,
    bias,
    spread,
    xall,
    psend,
    precv,
    mixall,
    osend,
    orecv,
    load_sem,
    x_sem,
    p_sem,
    m_sem,
    o_sem,
    send_sem,
):
    tp = lax.axis_index("tp")
    dp = lax.axis_index("dp")
    rows, width = tok_h.shape
    heads = width // HEAD
    pairs = width // 128
    tiles = HEAD * HEAD // 128
    cols = 4 * width

    def tp_peer(i):
        return lax.rem(tp + i, n)

    def dp_peer(i):
        return lax.rem(dp + i, n)

    def by_distance(i):
        half = lax.div(i + 1, 2)
        return lax.rem(tp + n + half * (2 * lax.rem(i, 2) - 1), n)

    barrier = pltpu.get_barrier_semaphore()

    def greet(i, carry):
        pl.semaphore_signal(barrier, inc=1, device_id={"tp": tp_peer(i)}, device_id_type=MESH)
        pl.semaphore_signal(barrier, inc=1, device_id={"dp": dp_peer(i)}, device_id_type=MESH)
        return carry

    lax.fori_loop(1, n, greet, 0)

    loads = [
        pltpu.make_async_copy(tok_h, xall.at[0, tp], load_sem.at[0]),
        pltpu.make_async_copy(gain_h, gain, load_sem.at[1]),
        pltpu.make_async_copy(ig_h, gate_in.at[0], load_sem.at[2]),
        pltpu.make_async_copy(fg_h, gate_in.at[1], load_sem.at[3]),
        pltpu.make_async_copy(fb_h, fb, load_sem.at[4]),
        pltpu.make_async_copy(mx_h, mx, load_sem.at[5]),
        pltpu.make_async_copy(nrm_h, nrm, load_sem.at[6]),
    ]
    for i, ref in enumerate((qw_h, kw_h, vw_h, ow_h)):
        loads.append(pltpu.make_async_copy(ref, w.at[i], load_sem.at[7 + i]))
    loads.append(pltpu.make_async_copy(mem_h, mem, load_sem.at[11]))
    loads.append(pltpu.make_async_copy(pw_h, pw, load_sem.at[12]))
    for copy in loads:
        copy.start()

    for c in range(HEAD * HEAD // 512):
        shape = (HEAD, 512)
        block = lane_iota(shape) + c * 512
        row = lax.broadcasted_iota(jnp.int32, shape, 0)
        hit = (block >= row * HEAD) & (block < row * HEAD + HEAD)
        spread[:, c * 512 : (c + 1) * 512] = jnp.where(hit, 1.0, 0.0).astype(BF16)
    for copy in loads[1:7]:
        copy.wait()
    lane = lane_iota((rows, 128))
    row8 = lax.broadcasted_iota(jnp.int32, (rows, 128), 0)
    low = lane < HEAD

    def per_head(values):
        wide = [jnp.broadcast_to(v, (rows, 128)) for v in values]
        return jnp.concatenate(
            [jnp.where(low, wide[2 * p], wide[2 * p + 1]) for p in range(pairs)], axis=1
        )

    def both_halves(x, h):
        part = x[:, (h // 2) * 128 : (h // 2 + 1) * 128]
        turned = pltpu.roll(part, HEAD, 1)
        return jnp.where(low, part, turned) if h % 2 == 0 else jnp.where(low, turned, part)

    eye = (lane_iota((rows, rows)) == lax.broadcasted_iota(jnp.int32, (rows, rows), 0))
    for l in range(layers):
        gate_w[l] = jnp.concatenate(
            [
                gate_in[0, l].astype(F32),
                gate_in[1, l].astype(F32),
                jnp.zeros((128 - 2 * heads, width), F32),
            ],
            axis=0,
        ).astype(BF16)
        old = mx[l]
        old_max[l] = per_head(
            [
                jnp.sum(
                    jnp.where(eye, jnp.broadcast_to(old[h : h + 1, :], (rows, rows)), 0.0),
                    axis=1,
                    keepdims=True,
                )
                for h in range(heads)
            ]
        )
        bias[l] = per_head(
            [jnp.broadcast_to(fb[l : l + 1, h : h + 1], (rows, 1)) for h in range(heads)]
        )

    with jax.named_scope("barrier"):
        pl.semaphore_wait(barrier, 2 * (n - 1))
        loads[0].wait()

    def send_rows(l):
        def far_first(k, carry):
            t = by_distance(n - k)
            pltpu.make_async_remote_copy(
                src_ref=xall.at[l, tp],
                dst_ref=xall.at[l, tp],
                send_sem=send_sem.at[l, 0],
                recv_sem=x_sem.at[l, tp],
                device_id={"tp": t},
                device_id_type=MESH,
            ).start()
            return carry

        lax.fori_loop(1, n, far_first, 0)

    send_rows(0)
    for copy in loads[7:]:
        copy.wait()

    for l in range(layers):

        def turn(r, carry):
            mem_t[l, r] = mem[l, pl.ds(r, rows, stride=heads * tiles), :]
            return carry

        lax.fori_loop(0, heads * tiles, turn, 0, unroll=8)

    for l in range(layers):
        gain_row = gain[l : l + 1, :]

        def project(k, carry):
            sources = [by_distance(k * BATCH + j) for j in range(BATCH)]
            for j, t in enumerate(sources):

                @pl.when(t != tp)
                def _(t=t):
                    with jax.named_scope(f"wait_x{l}"):
                        here = xall.at[l, t]
                        pltpu.make_async_copy(here, here, x_sem.at[l, t]).wait()

            x = jnp.concatenate([xall[l, t].astype(F32) for t in sources], axis=0)
            scaled = (x * gain_row).astype(BF16)
            square = jnp.sum(x * x, axis=1, keepdims=True)
            gates = lax.dot_general(
                scaled, gate_w[l], (((1,), (1,)), ((), ())), preferred_element_type=F32
            )
            lanes = lane_iota(gates.shape)
            gates = jnp.where(lanes == 2 * heads, jnp.broadcast_to(square, gates.shape), gates)
            upper = gates.astype(BF16).astype(F32)
            rest = pltpu.roll(gates - upper, 16, 1)
            parts = [dot(scaled, w[q, l]) for q in range(4)]
            parts.append(jnp.where(lanes < 16, upper, rest))
            for j, t in enumerate(sources):
                block = jnp.concatenate([p[j * rows : (j + 1) * rows] for p in parts], axis=1)
                psend[l, t] = block.astype(BF16)
            for t in sources:

                @pl.when(t == dp)
                def _(t=t):
                    precv[l, dp] = psend[l, t]

                @pl.when(t != dp)
                def _(t=t):
                    pltpu.make_async_remote_copy(
                        src_ref=psend.at[l, t],
                        dst_ref=precv.at[l, dp],
                        send_sem=send_sem.at[l, 1],
                        recv_sem=p_sem.at[l],
                        device_id={"dp": t},
                        device_id_type=MESH,
                    ).start()

            return carry

        lax.fori_loop(0, n // BATCH, project, 0)

        some = precv.at[l, pl.ds(0, n - 1)]
        with jax.named_scope(f"wait_p{l}"):
            pltpu.make_async_copy(some, some, p_sem.at[l]).wait()
        total = precv[l, 0].astype(F32)
        for s in range(1, n):
            total = total + precv[l, s].astype(F32)
        gates = total[:, cols:]
        gates = gates + pltpu.roll(gates, 128 - 16, 1)
        inv_rms = lax.rsqrt(gates[:, 2 * heads : 2 * heads + 1] / (width * n) + EPS)
        gates = gates * inv_rms
        stored = (total[:, :cols] * inv_rms).astype(BF16).astype(F32)
        query = stored[:, :width]
        keys = stored[:, width : 2 * width] * HEAD**-0.5
        values = stored[:, 2 * width : 3 * width]
        outgate = stored[:, 3 * width :]

        def stack(x):
            return jnp.concatenate(
                [x[:, h * HEAD : (h + 1) * HEAD] for h in range(heads)], axis=0
            ).astype(BF16)

        query_rows = stack(query)
        acc = [None] * heads
        chunk = 4
        for c in range(tiles // chunk):
            wide = dot(query_rows, spread[:, c * chunk * 128 : (c + 1) * chunk * 128])
            for j in range(chunk):
                for h in range(heads):
                    term = (
                        wide[h * rows : (h + 1) * rows, j * 128 : (j + 1) * 128]
                        * mem_t[l, (c * chunk + j) * heads + h]
                    )
                    acc[h] = term if acc[h] is None else acc[h] + term

        input_pre = per_head([gates[:, h : h + 1] for h in range(heads)])
        forget_pre = per_head([gates[:, heads + h : heads + h + 1] for h in range(heads)]) + bias[l]
        log_forget = jnp.minimum(forget_pre, 0.0) - jnp.log1p(jnp.exp(-jnp.abs(forget_pre)))
        carried = log_forget + old_max[l]
        new_max = jnp.maximum(carried, input_pre)
        keep = jnp.exp(carried - new_max)
        admit = jnp.exp(input_pre - new_max)
        normalizer = keep * nrm[l] + admit * keys

        def head_sum(x):
            return per_head(
                [
                    jnp.sum(x[:, h * HEAD : (h + 1) * HEAD], axis=1, keepdims=True)
                    for h in range(heads)
                ]
            )

        query_key = head_sum(query * keys)
        denominator = head_sum(query * normalizer)
        folded = [a + pltpu.roll(a, HEAD, 1) for a in acc]
        from_memory = jnp.concatenate(
            [jnp.where(low, folded[2 * p], folded[2 * p + 1]) for p in range(pairs)], axis=1
        )
        numerator = keep * from_memory + admit * query_key * values
        readout = numerator / jnp.maximum(jnp.abs(denominator), jnp.exp(-new_max))
        mixall[l, dp] = (readout * jax.nn.sigmoid(outgate)).astype(BF16)

        def send_mixed(i, carry):
            pltpu.make_async_remote_copy(
                src_ref=mixall.at[l, dp],
                dst_ref=mixall.at[l, dp],
                send_sem=send_sem.at[l, 2],
                recv_sem=m_sem.at[l, dp],
                device_id={"dp": dp_peer(i)},
                device_id_type=MESH,
            ).start()
            return carry

        with jax.named_scope(f"send_m{l}"):
            lax.fori_loop(1, n, send_mixed, 0)

        nrm_o[l] = normalizer
        key_rows = stack(keys)
        keep_h = [both_halves(keep, h) for h in range(heads)]
        value_h = [both_halves(admit * values, h) for h in range(heads)]
        for h in range(heads):
            peak = jnp.where(lane == row8, both_halves(new_max, h), 0.0)
            mx_o[l, h : h + 1, :] = jnp.sum(peak, axis=0, keepdims=True)[:, :rows]
        for c in range(tiles // chunk):
            wide = dot(key_rows, spread[:, c * chunk * 128 : (c + 1) * chunk * 128])
            for j in range(chunk):
                for h in range(heads):
                    r = (c * chunk + j) * heads + h
                    spread_key = wide[h * rows : (h + 1) * rows, j * 128 : (j + 1) * 128]
                    mem_o[l, pl.ds(r, rows, stride=heads * tiles), :] = (
                        keep_h[h] * mem_t[l, r] + spread_key * value_h[h]
                    )

        def leave(k, carry):
            homes = [by_distance(k * BATCH + j) for j in range(BATCH)]
            for t in homes:

                @pl.when(t != dp)
                def _(t=t):
                    with jax.named_scope(f"wait_m{l}"):
                        here = mixall.at[l, t]
                        pltpu.make_async_copy(here, here, m_sem.at[l, t]).wait()

            mixed = jnp.concatenate([mixall[l, t].astype(F32) for t in homes], axis=0)
            part = dot(mixed.astype(BF16), pw[l])
            for j, t in enumerate(homes):
                osend[l, t] = part[j * rows : (j + 1) * rows].astype(BF16)
            for t in homes:

                @pl.when(t == tp)
                def _(t=t):
                    orecv[l, tp] = osend[l, t]

                @pl.when(t != tp)
                def _(t=t):
                    pltpu.make_async_remote_copy(
                        src_ref=osend.at[l, t],
                        dst_ref=orecv.at[l, tp],
                        send_sem=send_sem.at[l, 3],
                        recv_sem=o_sem.at[l],
                        device_id={"tp": t},
                        device_id_type=MESH,
                    ).start()

            return carry

        lax.fori_loop(0, n // BATCH, leave, 0)

        some = orecv.at[l, pl.ds(0, n - 1)]
        with jax.named_scope(f"wait_o{l}"):
            pltpu.make_async_copy(some, some, o_sem.at[l]).wait()
        total = orecv[l, 0].astype(F32)
        for s in range(1, n):
            total = total + orecv[l, s].astype(F32)
        rows_out = (xall[l, tp].astype(F32) + total).astype(BF16)
        if l + 1 < layers:
            xall[l + 1, tp] = rows_out
            send_rows(l + 1)
        else:
            tok_o[...] = rows_out

    for l in range(layers):
        for k, buffer in enumerate((xall, psend, mixall, osend)):
            some = buffer.at[l, pl.ds(0, n - 1)]
            pltpu.make_async_copy(some, some, send_sem.at[l, k]).wait()


def put_out(*refs):
    sems = refs[8]
    copies = [pltpu.make_async_copy(refs[i], refs[4 + i], sems.at[i]) for i in range(4)]
    for copy in copies:
        copy.start()
    for copy in copies:
        copy.wait()


def per_device(
    n,
    tokens,
    norm_gain,
    query_weight,
    key_weight,
    value_weight,
    outgate_weight,
    input_gate_weight,
    forget_gate_weight,
    forget_bias,
    out_weight,
    memory_state,
    normalizer_state,
    maximum_state,
):
    rows, width = tokens.shape
    layers = norm_gain.shape[0]
    heads = width // HEAD
    tiles = HEAD * HEAD // 128
    vmem = pltpu.VMEM

    memory = memory_state.reshape(layers, rows, heads, tiles, 128).transpose(0, 1, 3, 2, 4)
    memory = memory.reshape(layers, rows * tiles * heads, 128)

    in_hbm = pl.BlockSpec(memory_space=pltpu.HBM)
    in_vmem = pl.BlockSpec(memory_space=pltpu.VMEM)
    block = 4 * width + 128
    tokens_out, memory, normalizer, maximum = pl.pallas_call(
        functools.partial(kernel, n, layers),
        out_shape=(
            pltpu.VMEM((rows, width), BF16),
            pltpu.VMEM(memory.shape, F32),
            pltpu.VMEM((layers, rows, width), F32),
            pltpu.VMEM((layers, heads, rows), F32),
        ),
        in_specs=[in_hbm] * 13,
        out_specs=(in_vmem,) * 4,
        scratch_shapes=[
            vmem((layers, width), F32),
            vmem((4, layers, width, width), BF16),
            vmem((2, layers, heads, width), BF16),
            vmem((layers, 128, width), BF16),
            vmem((layers, heads), F32),
            vmem((layers, width, width), BF16),
            vmem(memory.shape, F32),
            vmem((layers, heads * tiles, rows, 128), F32),
            vmem((layers, rows, width), F32),
            vmem((layers, heads, rows), F32),
            vmem((layers, rows, width), F32),
            vmem((layers, rows, width), F32),
            vmem((HEAD, HEAD * HEAD), BF16),
            vmem((layers, n, rows, width), BF16),
            vmem((layers, n, rows, block), BF16),
            vmem((layers, n, rows, block), BF16),
            vmem((layers, n, rows, width), BF16),
            vmem((layers, n, rows, width), BF16),
            vmem((layers, n, rows, width), BF16),
            pltpu.SemaphoreType.DMA((13,)),
            pltpu.SemaphoreType.DMA((layers, n)),
            pltpu.SemaphoreType.DMA((layers,)),
            pltpu.SemaphoreType.DMA((layers, n)),
            pltpu.SemaphoreType.DMA((layers,)),
            pltpu.SemaphoreType.DMA((layers, 4)),
        ],
        compiler_params=pltpu.CompilerParams(
            collective_id=0, has_side_effects=True, vmem_limit_bytes=48 * 1024 * 1024
        ),
        name="cells",
    )(
        *(
            pltpu.with_memory_space_constraint(a, pltpu.HBM)
            for a in (
                tokens,
                norm_gain,
                query_weight,
                key_weight,
                value_weight,
                outgate_weight,
                jnp.swapaxes(input_gate_weight, 1, 2),
                jnp.swapaxes(forget_gate_weight, 1, 2),
                forget_bias,
                out_weight,
                memory,
                normalizer_state,
                jnp.swapaxes(maximum_state, 1, 2),
            )
        )
    )
    results = (tokens_out, memory, normalizer, maximum)
    tokens_out, memory, normalizer, maximum = pl.pallas_call(
        put_out,
        out_shape=tuple(jax.ShapeDtypeStruct(r.shape, r.dtype) for r in results),
        in_specs=[in_vmem] * 4,
        out_specs=(in_hbm,) * 4,
        scratch_shapes=[pltpu.SemaphoreType.DMA((4,))],
        compiler_params=pltpu.CompilerParams(vmem_limit_bytes=4 * 1024 * 1024),
        name="put_out",
    )(*results)
    memory = memory.reshape(layers, rows, tiles, heads, 128).transpose(0, 1, 3, 2, 4)
    return (
        tokens_out,
        memory.reshape(layers, rows, heads, HEAD * HEAD),
        normalizer,
        jnp.swapaxes(maximum, 1, 2),
    )


def solution(mesh):
    n = mesh.shape["tp"]
    assert mesh.shape["dp"] == n
    in_specs = (
        P(("grp", "tp"), "dp"),
        P(None, "dp"),
        P(None, "dp", "tp"),
        P(None, "dp", "tp"),
        P(None, "dp", "tp"),
        P(None, "dp", "tp"),
        P(None, "dp", "tp"),
        P(None, "dp", "tp"),
        P(None, "tp"),
        P(None, "tp", "dp"),
        P(None, ("grp", "dp"), "tp", None),
        P(None, ("grp", "dp"), "tp"),
        P(None, ("grp", "dp"), "tp"),
    )
    out_specs = (
        P(("grp", "tp"), "dp"),
        P(None, ("grp", "dp"), "tp", None),
        P(None, ("grp", "dp"), "tp"),
        P(None, ("grp", "dp"), "tp"),
    )
    return jax.shard_map(
        functools.partial(per_device, n),
        mesh=mesh,
        in_specs=in_specs,
        out_specs=out_specs,
        check_vma=False,
    )
```

time: 199 us -> 106 us (0.53)
  Pallas kernels: 0 us -> 104 us
  starting transfers between devices: 64 us -> 0 us
  waiting for transfers between devices: 58.4 us -> 0 us
  blocking collectives: 46.8 us -> 0 us
  local copies, waits for them, and re-layouts: 18 us -> 0 us
  other arithmetic: 6.93 us -> 0 us
  matrix products: 3.3 us -> 0 us
    pallas_call x0 -> x2, Pallas kernels: none -> 104 us  [the longest x1 103 us: per_device(): pl.pallas_call(functools.partial(kernel, n, layers), out_shape=(pltpu.VME...]
    all_to_all x5 -> x0, starting transfers between devices: 64 us -> none  [the longest x2 48.4 us: from_everyone(): return lax.all_to_all(copies, axis, split_axis=0, concat_axis=0, tiled=True)]
    all_to_all x5 -> x0, waiting for transfers between devices: 58.4 us -> none  [the longest x3 40.9 us: sent_and_summed(): lax.all_to_all(tiles, axis, split_axis=0, concat_axis=0, tiled=True)]
    all_to_all x3 -> x0, blocking collectives: 46.8 us -> none  [the longest x2 30.4 us: from_everyone(): return lax.all_to_all(copies, axis, split_axis=0, concat_axis=0, tiled=True)]
    unnamed x30 -> x0, local copies, waits for them, and re-layouts: 4.68 us -> none
    dot_general x8 -> x0, matrix products: 3.3 us -> none  [the longest x2 1.55 us: cell_layer(): jnp.einsum('bhd,bhde->bhe', query_vec, memory, precision=lax.Precision.HI...]
    slice x11 -> x0, local copies, waits for them, and re-layouts: 2.96 us -> none  [the longest x4 1.22 us: cell_layer(): query_vec = stored[:, 0:width].reshape(shape)]
    another operation x3 -> x0, other arithmetic: 2.41 us -> none  [the longest x1 1.21 us: per_device(): jnp.stack([memory_first, memory_second])]
  transfers between devices with their start and end apart: 5 -> 0, of which waited for: 5 -> 0; matrix products, arithmetic and copies ran while one was open for 3% -> 0% of each run, Pallas kernels for 0% -> 0%
where the time goes in v1:
time: 106 us; the launch traced here: 105 us
  Pallas kernels  104 us (98%)
    pallas_call x1, Pallas kernels, per_device(): pl.pallas_call(functools.partial(kernel, n, layers), out_shape=(pltpu.VME...  103 us

profile of v1, /device:TPU:80, one launch (start us, length us, event | category | flops | bytes accessed | tf_op | source)
XLA Modules:
  0.0 104.7 jit_solution(15088342134753472453)
XLA Ops:
  0.6 103.0 %cells.1 = (bf16[8,256]{1,0:T(8,128)(2,1)S(1)}, f32[2,1024,128]{2,1,0:T(8,128)S(1)}, f32[2,8,256]{2,1,0:T(8,128)S(1)}, f32[2,4,8]{2,1,0:T(4,128)S(1)}) custom-call(bf16[8,256]{1,0:T(8,128)(2,1)} %tok_h.1, f32[2,256]{1,0:T(2,128)} %gain_h.1, bf16[2,256,256]{2,1,0:T(8,128)(2,1)} %qw_h.1, bf16[2,256,256]{2,1,0:T(8,128)(2,1)} %kw_h.1, ...), custom_call_target="tpu_custom_call" | custom-call | tf_op jit(solution)/shard_map/cells/pallas_call | solution.py:426
  103.6 1.0 put_out.1

commit v2 on v1

--- a/solution.py
+++ b/solution.py
@@ -57,6 +57,8 @@
     bias,
     spread,
     xall,
+    pfull,
+    pother,
     psend,
     precv,
     mixall,
@@ -64,6 +66,7 @@
     orecv,
     load_sem,
     x_sem,
+    c_sem,
     p_sem,
     m_sem,
     o_sem,
@@ -86,6 +89,17 @@
     def by_distance(i):
         half = lax.div(i + 1, 2)
         return lax.rem(tp + n + half * (2 * lax.rem(i, 2) - 1), n)
+
+    core = lax.rem(dp, 2)
+    chip = lax.div(dp, 2)
+    sibling = dp + 1 - 2 * core
+    odd = lax.rem(tp + core, 2)
+
+    def of_core(k, parity):
+        return [
+            by_distance(k * BATCH + lax.select(parity == 0, even, uneven))
+            for even, uneven in ((0, 1), (3, 2))
+        ]
 
     barrier = pltpu.get_barrier_semaphore()
 
@@ -194,9 +208,9 @@
     for l in range(layers):
         gain_row = gain[l : l + 1, :]
 
-        def project(k, carry):
+        def project(k):
             sources = [by_distance(k * BATCH + j) for j in range(BATCH)]
-            for j, t in enumerate(sources):
+            for t in sources:
 
                 @pl.when(t != tp)
                 def _(t=t):
@@ -210,41 +224,63 @@
             gates = lax.dot_general(
                 scaled, gate_w[l], (((1,), (1,)), ((), ())), preferred_element_type=F32
             )
-            lanes = lane_iota(gates.shape)
-            gates = jnp.where(lanes == 2 * heads, jnp.broadcast_to(square, gates.shape), gates)
-            upper = gates.astype(BF16).astype(F32)
-            rest = pltpu.roll(gates - upper, 16, 1)
-            parts = [dot(scaled, w[q, l]) for q in range(4)]
-            parts.append(jnp.where(lanes < 16, upper, rest))
+            gates = jnp.where(
+                lane_iota(gates.shape) == 2 * heads, jnp.broadcast_to(square, gates.shape), gates
+            )
+            parts = [dot(scaled, w[q, l]) for q in range(4)] + [gates]
             for j, t in enumerate(sources):
-                block = jnp.concatenate([p[j * rows : (j + 1) * rows] for p in parts], axis=1)
+                pfull[l, t] = jnp.concatenate(
+                    [p[j * rows : (j + 1) * rows] for p in parts], axis=1
+                )
+            for t in of_core(k, 1 - odd):
+                pltpu.make_async_remote_copy(
+                    src_ref=pfull.at[l, t],
+                    dst_ref=pother.at[l, t],
+                    send_sem=send_sem.at[l, 4],
+                    recv_sem=c_sem.at[l, t],
+                    device_id={"dp": sibling},
+                    device_id_type=MESH,
+                ).start()
+
+        def pass_on(k):
+            for t in of_core(k, odd):
+                with jax.named_scope(f"wait_c{l}"):
+                    there = pother.at[l, t]
+                    pltpu.make_async_copy(there, there, c_sem.at[l, t]).wait()
+                both = pfull[l, t] + pother[l, t]
+                gates = both[:, cols:]
+                upper = gates.astype(BF16).astype(F32)
+                rest = pltpu.roll(gates - upper, 16, 1)
+                gates = jnp.where(lane < 16, upper, rest)
+                block = jnp.concatenate([both[:, :cols], gates], axis=1)
                 psend[l, t] = block.astype(BF16)
-            for t in sources:
 
                 @pl.when(t == dp)
                 def _(t=t):
-                    precv[l, dp] = psend[l, t]
+                    precv[l, chip] = psend[l, t]
 
                 @pl.when(t != dp)
                 def _(t=t):
                     pltpu.make_async_remote_copy(
                         src_ref=psend.at[l, t],
-                        dst_ref=precv.at[l, dp],
+                        dst_ref=precv.at[l, chip],
                         send_sem=send_sem.at[l, 1],
                         recv_sem=p_sem.at[l],
                         device_id={"dp": t},
                         device_id_type=MESH,
                     ).start()
 
-            return carry
-
-        lax.fori_loop(0, n // BATCH, project, 0)
-
-        some = precv.at[l, pl.ds(0, n - 1)]
+        for k in range(n // BATCH):
+            project(k)
+            if k > 0:
+                pass_on(k - 1)
+        pass_on(n // BATCH - 1)
+
+        some = precv.at[l, pl.ds(0, n // 2 - 1)]
         with jax.named_scope(f"wait_p{l}"):
             pltpu.make_async_copy(some, some, p_sem.at[l]).wait()
         total = precv[l, 0].astype(F32)
-        for s in range(1, n):
+        for s in range(1, n // 2):
             total = total + precv[l, s].astype(F32)
         gates = total[:, cols:]
         gates = gates + pltpu.roll(gates, 128 - 16, 1)
@@ -381,8 +417,9 @@
             tok_o[...] = rows_out
 
     for l in range(layers):
-        for k, buffer in enumerate((xall, psend, mixall, osend)):
-            some = buffer.at[l, pl.ds(0, n - 1)]
+        sent = ((xall, n - 1), (psend, n // 2 - 1), (mixall, n - 1), (osend, n - 1), (pfull, n // 2))
+        for k, (buffer, count) in enumerate(sent):
+            some = buffer.at[l, pl.ds(0, count)]
             pltpu.make_async_copy(some, some, send_sem.at[l, k]).wait()
 
 
@@ -448,17 +485,20 @@
             vmem((layers, rows, width), F32),
             vmem((HEAD, HEAD * HEAD), BF16),
             vmem((layers, n, rows, width), BF16),
+            vmem((layers, n, rows, block), F32),
+            vmem((layers, n, rows, block), F32),
             vmem((layers, n, rows, block), BF16),
-            vmem((layers, n, rows, block), BF16),
+            vmem((layers, n // 2, rows, block), BF16),
             vmem((layers, n, rows, width), BF16),
             vmem((layers, n, rows, width), BF16),
             vmem((layers, n, rows, width), BF16),
             pltpu.SemaphoreType.DMA((13,)),
             pltpu.SemaphoreType.DMA((layers, n)),
+            pltpu.SemaphoreType.DMA((layers, n)),
             pltpu.SemaphoreType.DMA((layers,)),
             pltpu.SemaphoreType.DMA((layers, n)),
             pltpu.SemaphoreType.DMA((layers,)),
-            pltpu.SemaphoreType.DMA((layers, 4)),
+            pltpu.SemaphoreType.DMA((layers, 5)),
         ],
         compiler_params=pltpu.CompilerParams(
             collective_id=0, has_side_effects=True, vmem_limit_bytes=48 * 1024 * 1024

time: 106 us -> 105 us (level)
  no operation moved by 1% of the time
where the time goes in v2:
time: 105 us; the launch traced here: 104 us
  Pallas kernels  103 us (98%)
    pallas_call x1, Pallas kernels, per_device(): pl.pallas_call(functools.partial(kernel, n, layers), out_shape=(pltpu.VME...  102 us

profile of v2, /device:TPU:80, one launch (start us, length us, event | category | flops | bytes accessed | tf_op | source)
XLA Modules:
  0.0 104.1 jit_solution(7934911723052874870)
XLA Ops:
  0.6 102.4 %cells.1 = (bf16[8,256]{1,0:T(8,128)(2,1)S(1)}, f32[2,1024,128]{2,1,0:T(8,128)S(1)}, f32[2,8,256]{2,1,0:T(8,128)S(1)}, f32[2,4,8]{2,1,0:T(4,128)S(1)}) custom-call(bf16[8,256]{1,0:T(8,128)(2,1)} %tok_h.1, f32[2,256]{1,0:T(2,128)} %gain_h.1, bf16[2,256,256]{2,1,0:T(8,128)(2,1)} %qw_h.1, bf16[2,256,256]{2,1,0:T(8,128)(2,1)} %kw_h.1, ...), custom_call_target="tpu_custom_call" | custom-call | tf_op jit(solution)/shard_map/cells/pallas_call | solution.py:463
  103.1 1.0 put_out.1

commit v3 on v2

--- a/solution.py
+++ b/solution.py
@@ -10,6 +10,7 @@
 HEAD = 64
 EPS = 1e-06
 BATCH = 4
+HUB = 1
 MESH = pl.DeviceIdType.MESH
 F32 = jnp.float32
 BF16 = jnp.bfloat16
@@ -71,6 +72,9 @@
     m_sem,
     o_sem,
     send_sem,
+    hub_sem,
+    plane_sem,
+    ready_sem,
 ):
     tp = lax.axis_index("tp")
     dp = lax.axis_index("dp")
@@ -80,9 +84,6 @@
     tiles = HEAD * HEAD // 128
     cols = 4 * width
 
-    def tp_peer(i):
-        return lax.rem(tp + i, n)
-
     def dp_peer(i):
         return lax.rem(dp + i, n)
 
@@ -90,25 +91,49 @@
         half = lax.div(i + 1, 2)
         return lax.rem(tp + n + half * (2 * lax.rem(i, 2) - 1), n)
 
+    def arrival(i):
+        return lax.select(i < n - 2, HUB + i, lax.select(i == n - 2, 0, n - 1))
+
+    def by_owner(i):
+        return lax.rem(by_distance(lax.div(i, 2)) + (n // 2) * lax.rem(i, 2), n)
+
+    opposite = lax.rem(tp + n // 2, n)
     core = lax.rem(dp, 2)
     chip = lax.div(dp, 2)
     sibling = dp + 1 - 2 * core
     odd = lax.rem(tp + core, 2)
 
-    def of_core(k, parity):
-        return [
-            by_distance(k * BATCH + lax.select(parity == 0, even, uneven))
-            for even, uneven in ((0, 1), (3, 2))
-        ]
+    def batch_of(l, k):
+        places = range(k * BATCH, (k + 1) * BATCH)
+        where = arrival if l == 0 else by_owner
+        return [where(i) for i in places]
+
+    def of_core(l, k, mine):
+        if l == 0:
+            order = [(HUB + i) % 2 if i < n - 2 else (0, 1)[i - n + 2] for i in range(n)]
+            flag = core
+        else:
+            order = [((i // 2 + 1) // 2) % 2 for i in range(n)]
+            flag = odd
+        places = range(k * BATCH, (k + 1) * BATCH)
+        even = [i for i in places if order[i] == 0]
+        uneven = [i for i in places if order[i] == 1]
+        flag = flag if mine else 1 - flag
+        where = arrival if l == 0 else by_owner
+        return [where(lax.select(flag == 0, e, u)) for e, u in zip(even, uneven, strict=True)]
 
     barrier = pltpu.get_barrier_semaphore()
-
-    def greet(i, carry):
-        pl.semaphore_signal(barrier, inc=1, device_id={"tp": tp_peer(i)}, device_id_type=MESH)
-        pl.semaphore_signal(barrier, inc=1, device_id={"dp": dp_peer(i)}, device_id_type=MESH)
-        return carry
-
-    lax.fori_loop(1, n, greet, 0)
+    at_hub = tp == HUB
+
+    @pl.when(at_hub)
+    def _():
+        def greet(i, carry):
+            pl.semaphore_signal(barrier, inc=1, device_id={"dp": dp_peer(i)}, device_id_type=MESH)
+            there = {"tp": lax.rem(tp + i, n)}
+            pl.semaphore_signal(barrier, inc=1, device_id=there, device_id_type=MESH)
+            return carry
+
+        lax.fori_loop(1, n, greet, 0)
 
     loads = [
         pltpu.make_async_copy(tok_h, xall.at[0, tp], load_sem.at[0]),
@@ -125,6 +150,38 @@
     loads.append(pltpu.make_async_copy(pw_h, pw, load_sem.at[12]))
     for copy in loads:
         copy.start()
+
+    with jax.named_scope("barrier"):
+        pl.semaphore_wait(barrier, lax.select(at_hub, n - 1, 1))
+        loads[0].wait()
+
+    def row_copy(l, block, t, sem):
+        return pltpu.make_async_remote_copy(
+            src_ref=xall.at[l, block],
+            dst_ref=xall.at[l, block],
+            send_sem=sem,
+            recv_sem=x_sem.at[l, block],
+            device_id={"tp": t},
+            device_id_type=MESH,
+        )
+
+    def wait_rows(l, block):
+        with jax.named_scope(f"wait_x{l}"):
+            here = xall.at[l, block]
+            pltpu.make_async_copy(here, here, x_sem.at[l, block]).wait()
+
+    def send_rows(l):
+        def far_first(k, carry):
+            t = by_distance(n // 2 - k)
+            row_copy(l, tp, t, send_sem.at[l, 0]).start()
+            row_copy(l, opposite, t, send_sem.at[l, 0]).start()
+            return carry
+
+        lax.fori_loop(1, n // 2, far_first, 0)
+
+    @pl.when(jnp.logical_not(at_hub))
+    def _():
+        row_copy(0, tp, HUB, send_sem.at[0, 0]).start()
 
     for c in range(HEAD * HEAD // 512):
         shape = (HEAD, 512)
@@ -174,27 +231,7 @@
             [jnp.broadcast_to(fb[l : l + 1, h : h + 1], (rows, 1)) for h in range(heads)]
         )
 
-    with jax.named_scope("barrier"):
-        pl.semaphore_wait(barrier, 2 * (n - 1))
-        loads[0].wait()
-
-    def send_rows(l):
-        def far_first(k, carry):
-            t = by_distance(n - k)
-            pltpu.make_async_remote_copy(
-                src_ref=xall.at[l, tp],
-                dst_ref=xall.at[l, tp],
-                send_sem=send_sem.at[l, 0],
-                recv_sem=x_sem.at[l, tp],
-                device_id={"tp": t},
-                device_id_type=MESH,
-            ).start()
-            return carry
-
-        lax.fori_loop(1, n, far_first, 0)
-
-    send_rows(0)
-    for copy in loads[7:]:
+    for copy in loads[7:12]:
         copy.wait()
 
     for l in range(layers):
@@ -205,18 +242,59 @@
 
         lax.fori_loop(0, heads * tiles, turn, 0, unroll=8)
 
+    @pl.when(at_hub)
+    def _():
+        def relay(j, carry):
+            block = arrival(j + 1)
+            wait_rows(0, block)
+
+            def tell(i, c):
+                there = {"dp": dp_peer(i)}
+                pl.semaphore_signal(
+                    plane_sem.at[block], inc=1, device_id=there, device_id_type=MESH
+                )
+                return c
+
+            lax.fori_loop(1, n, tell, 0)
+
+            def to_known(q, c):
+                t = arrival(q)
+                row_copy(0, block, t, hub_sem.at[t]).start()
+                return c
+
+            lax.fori_loop(1, j + 1, to_known, 0)
+
+            def catch_up(q, c):
+                row_copy(0, arrival(q), block, hub_sem.at[block]).start()
+                return c
+
+            lax.fori_loop(0, j + 1, catch_up, 0)
+
+            @pl.when(j > 0)
+            def _():
+                settle(j - 1)
+
+            return carry
+
+        def settle(j):
+            t = arrival(j + 1)
+            pl.semaphore_wait(plane_sem.at[t], n - 1)
+            pl.semaphore_signal(ready_sem, inc=1, device_id={"tp": t}, device_id_type=MESH)
+
+        lax.fori_loop(0, n - 1, relay, 0)
+        settle(n - 2)
+
+    loads[12].wait()
+
     for l in range(layers):
         gain_row = gain[l : l + 1, :]
 
         def project(k):
-            sources = [by_distance(k * BATCH + j) for j in range(BATCH)]
+            sources = batch_of(l, k)
             for t in sources:
-
-                @pl.when(t != tp)
+                @pl.when((t != tp) & (jnp.logical_not(at_hub) if l == 0 else t != opposite))
                 def _(t=t):
-                    with jax.named_scope(f"wait_x{l}"):
-                        here = xall.at[l, t]
-                        pltpu.make_async_copy(here, here, x_sem.at[l, t]).wait()
+                    wait_rows(l, t)
 
             x = jnp.concatenate([xall[l, t].astype(F32) for t in sources], axis=0)
             scaled = (x * gain_row).astype(BF16)
@@ -232,7 +310,8 @@
                 pfull[l, t] = jnp.concatenate(
                     [p[j * rows : (j + 1) * rows] for p in parts], axis=1
                 )
-            for t in of_core(k, 1 - odd):
+        def give(k):
+            for t in of_core(l, k, False):
                 pltpu.make_async_remote_copy(
                     src_ref=pfull.at[l, t],
                     dst_ref=pother.at[l, t],
@@ -243,7 +322,7 @@
                 ).start()
 
         def pass_on(k):
-            for t in of_core(k, odd):
+            for t in of_core(l, k, True):
                 with jax.named_scope(f"wait_c{l}"):
                     there = pother.at[l, t]
                     pltpu.make_async_copy(there, there, c_sem.at[l, t]).wait()
@@ -270,11 +349,29 @@
                         device_id_type=MESH,
                     ).start()
 
-        for k in range(n // BATCH):
-            project(k)
-            if k > 0:
-                pass_on(k - 1)
-        pass_on(n // BATCH - 1)
+        last = n // BATCH - 1
+        if l == 0:
+            for k in range(last):
+                project(k)
+
+            @pl.when(jnp.logical_not(at_hub))
+            def _():
+                with jax.named_scope("ready"):
+                    pl.semaphore_wait(ready_sem, 1)
+
+            for k in range(last):
+                give(k)
+            for k in range(last):
+                pass_on(k)
+            project(last)
+            give(last)
+        else:
+            for k in range(last + 1):
+                project(k)
+                give(k)
+                if k > 0:
+                    pass_on(k - 1)
+        pass_on(last)
 
         some = precv.at[l, pl.ds(0, n // 2 - 1)]
         with jax.named_scope(f"wait_p{l}"):
@@ -337,7 +434,9 @@
         readout = numerator / jnp.maximum(jnp.abs(denominator), jnp.exp(-new_max))
         mixall[l, dp] = (readout * jax.nn.sigmoid(outgate)).astype(BF16)
 
-        def send_mixed(i, carry):
+        def send_mixed(k, carry):
+            half = lax.div(k, 2)
+            i = lax.select(lax.rem(k, 2) == 0, n // 2 - half, n // 2 + half)
             pltpu.make_async_remote_copy(
                 src_ref=mixall.at[l, dp],
                 dst_ref=mixall.at[l, dp],
@@ -368,8 +467,15 @@
                         keep_h[h] * mem_t[l, r] + spread_key * value_h[h]
                     )
 
+        owners = 2 if l + 1 < layers else 1
+
         def leave(k, carry):
             homes = [by_distance(k * BATCH + j) for j in range(BATCH)]
+            if l == 0:
+                homes = [
+                    lax.select(tp == n - 1, by_distance(n - 1 - i), arrival(i))
+                    for i in (k * BATCH + j for j in range(BATCH))
+                ]
             for t in homes:
 
                 @pl.when(t != dp)
@@ -382,50 +488,83 @@
             part = dot(mixed.astype(BF16), pw[l])
             for j, t in enumerate(homes):
                 osend[l, t] = part[j * rows : (j + 1) * rows].astype(BF16)
-            for t in homes:
-
-                @pl.when(t == tp)
-                def _(t=t):
-                    orecv[l, tp] = osend[l, t]
-
-                @pl.when(t != tp)
-                def _(t=t):
-                    pltpu.make_async_remote_copy(
-                        src_ref=osend.at[l, t],
-                        dst_ref=orecv.at[l, tp],
-                        send_sem=send_sem.at[l, 3],
-                        recv_sem=o_sem.at[l],
-                        device_id={"tp": t},
-                        device_id_type=MESH,
-                    ).start()
+            for t in reversed(homes):
+
+                for owner in range(owners):
+                    home = lax.rem(t + owner * (n // 2), n)
+
+                    @pl.when(home == tp)
+                    def _(t=t, owner=owner):
+                        orecv[l, owner, tp] = osend[l, t]
+
+                    @pl.when(home != tp)
+                    def _(t=t, owner=owner, home=home):
+                        pltpu.make_async_remote_copy(
+                            src_ref=osend.at[l, t],
+                            dst_ref=orecv.at[l, owner, tp],
+                            send_sem=send_sem.at[l, 3 + 2 * owner],
+                            recv_sem=o_sem.at[l, owner],
+                            device_id={"tp": home},
+                            device_id_type=MESH,
+                        ).start()
 
             return carry
 
         lax.fori_loop(0, n // BATCH, leave, 0)
 
-        some = orecv.at[l, pl.ds(0, n - 1)]
-        with jax.named_scope(f"wait_o{l}"):
-            pltpu.make_async_copy(some, some, o_sem.at[l]).wait()
-        total = orecv[l, 0].astype(F32)
-        for s in range(1, n):
-            total = total + orecv[l, s].astype(F32)
-        rows_out = (xall[l, tp].astype(F32) + total).astype(BF16)
+        for owner in range(owners):
+            some = orecv.at[l, owner, pl.ds(0, n - 1)]
+            with jax.named_scope(f"wait_o{l}"):
+                pltpu.make_async_copy(some, some, o_sem.at[l, owner]).wait()
+        for owner in range(owners):
+            home = (tp, opposite)[owner]
+            total = orecv[l, owner, 0].astype(F32)
+            for s in range(1, n):
+                total = total + orecv[l, owner, s].astype(F32)
+            rows_out = (xall[l, home].astype(F32) + total).astype(BF16)
+            if l + 1 < layers:
+                xall[l + 1, home] = rows_out
+            else:
+                tok_o[...] = rows_out
         if l + 1 < layers:
-            xall[l + 1, tp] = rows_out
             send_rows(l + 1)
-        else:
-            tok_o[...] = rows_out
 
     for l in range(layers):
-        sent = ((xall, n - 1), (psend, n // 2 - 1), (mixall, n - 1), (osend, n - 1), (pfull, n // 2))
+        sent = [(xall, n - 2), (psend, n // 2 - 1), (mixall, n - 1), (osend, n - 1), (pfull, n // 2)]
+        if l + 1 < layers:
+            sent.append((osend, n - 1))
         for k, (buffer, count) in enumerate(sent):
             some = buffer.at[l, pl.ds(0, count)]
-            pltpu.make_async_copy(some, some, send_sem.at[l, k]).wait()
+            if l > 0 or k > 0:
+                pltpu.make_async_copy(some, some, send_sem.at[l, k]).wait()
+
+    @pl.when(jnp.logical_not(at_hub))
+    def _():
+        row_copy(0, tp, HUB, send_sem.at[0, 0]).wait_send()
+
+    @pl.when(at_hub)
+    def _():
+        def handed_on(j, carry):
+            some = xall.at[0, pl.ds(0, n - 1)]
+            pltpu.make_async_copy(some, some, hub_sem.at[arrival(j + 1)]).wait()
+            return carry
+
+        lax.fori_loop(0, n - 1, handed_on, 0)
 
 
 def put_out(*refs):
     sems = refs[8]
-    copies = [pltpu.make_async_copy(refs[i], refs[4 + i], sems.at[i]) for i in range(4)]
+    pieces = 8
+    copies = []
+    for src, dst in zip(refs[:4], refs[4:8], strict=True):
+        if src.ndim < 3 or src.shape[1] < 1024:
+            copies.append((src, dst))
+            continue
+        step = src.shape[1] * src.shape[0] // pieces
+        for at in range(0, src.shape[1], step):
+            for l in range(src.shape[0]):
+                copies.append((src.at[l, at : at + step], dst.at[l, at : at + step]))
+    copies = [pltpu.make_async_copy(*c, sems.at[i]) for i, c in enumerate(copies)]
     for copy in copies:
         copy.start()
     for copy in copies:
@@ -491,14 +630,17 @@
             vmem((layers, n // 2, rows, block), BF16),
             vmem((layers, n, rows, width), BF16),
             vmem((layers, n, rows, width), BF16),
-            vmem((layers, n, rows, width), BF16),
+            vmem((layers, 2, n, rows, width), BF16),
             pltpu.SemaphoreType.DMA((13,)),
             pltpu.SemaphoreType.DMA((layers, n)),
             pltpu.SemaphoreType.DMA((layers, n)),
             pltpu.SemaphoreType.DMA((layers,)),
             pltpu.SemaphoreType.DMA((layers, n)),
-            pltpu.SemaphoreType.DMA((layers,)),
-            pltpu.SemaphoreType.DMA((layers, 5)),
+            pltpu.SemaphoreType.DMA((layers, 2)),
+            pltpu.SemaphoreType.DMA((layers, 6)),
+            pltpu.SemaphoreType.DMA((n,)),
+            pltpu.SemaphoreType.REGULAR((n,)),
+            pltpu.SemaphoreType.REGULAR,
         ],
         compiler_params=pltpu.CompilerParams(
             collective_id=0, has_side_effects=True, vmem_limit_bytes=48 * 1024 * 1024
@@ -530,7 +672,7 @@
         out_shape=tuple(jax.ShapeDtypeStruct(r.shape, r.dtype) for r in results),
         in_specs=[in_vmem] * 4,
         out_specs=(in_hbm,) * 4,
-        scratch_shapes=[pltpu.SemaphoreType.DMA((4,))],
+        scratch_shapes=[pltpu.SemaphoreType.DMA((11,))],
         compiler_params=pltpu.CompilerParams(vmem_limit_bytes=4 * 1024 * 1024),
         name="put_out",
     )(*results)

time: 105 us -> 104 us (level); the launches traced: 104 us -> 104 us
  no operation moved by 1% of the time
where the time goes in v3:
time: 104 us
  Pallas kernels  104 us (100%)
    pallas_call x1, Pallas kernels, per_device(): pl.pallas_call(functools.partial(kernel, n, layers), out_shape=(pltpu.VME...  102 us

profile of v3, /device:TPU:80, one launch (start us, length us, event | category | flops | bytes accessed | tf_op | source)
XLA Modules:
  0.0 104.2 jit_solution(6844951363341016599)
XLA Ops:
  0.6 102.4 %cells.1 = (bf16[8,256]{1,0:T(8,128)(2,1)S(1)}, f32[2,1024,128]{2,1,0:T(8,128)S(1)}, f32[2,8,256]{2,1,0:T(8,128)S(1)}, f32[2,4,8]{2,1,0:T(4,128)S(1)}) custom-call(bf16[8,256]{1,0:T(8,128)(2,1)} %tok_h.1, f32[2,256]{1,0:T(2,128)} %gain_h.1, bf16[2,256,256]{2,1,0:T(8,128)(2,1)} %qw_h.1, bf16[2,256,256]{2,1,0:T(8,128)(2,1)} %kw_h.1, ...), custom_call_target="tpu_custom_call" | custom-call | tf_op jit(solution)/shard_map/cells/pallas_call | solution.py:602
  103.1 1.1 %put_out.1 = (bf16[8,256]{1,0:T(8,128)(2,1)}, f32[2,1024,128]{2,1,0:T(8,128)}, f32[2,8,256]{2,1,0:T(8,128)}, f32[2,4,8]{2,1,0:T(4,128)}) custom-call(bf16[8,256]{1,0:T(8,128)(2,1)S(1)} %get-tuple-element.12.refs_0_, f32[2,1024,128]{2,1,0:T(8,128)S(1)} %get-tuple-element.13.refs_1_, f32[2,8,256]{2,1,0:T(8,128)S(1)} %get-tuple-element.14.refs_2_, ...), custom_call_target="tpu_custom_call" | custom-call | tf_op jit(solution)/shard_map/put_out/pallas_call | solution.py:670

commit v4 on v3

--- a/solution.py
+++ b/solution.py
@@ -94,10 +94,6 @@
     def arrival(i):
         return lax.select(i < n - 2, HUB + i, lax.select(i == n - 2, 0, n - 1))
 
-    def by_owner(i):
-        return lax.rem(by_distance(lax.div(i, 2)) + (n // 2) * lax.rem(i, 2), n)
-
-    opposite = lax.rem(tp + n // 2, n)
     core = lax.rem(dp, 2)
     chip = lax.div(dp, 2)
     sibling = dp + 1 - 2 * core
@@ -105,21 +101,22 @@
 
     def batch_of(l, k):
         places = range(k * BATCH, (k + 1) * BATCH)
-        where = arrival if l == 0 else by_owner
-        return [where(i) for i in places]
+        if l == 0:
+            return [arrival(i) for i in places]
+        return [by_distance(i) for i in places]
 
     def of_core(l, k, mine):
         if l == 0:
             order = [(HUB + i) % 2 if i < n - 2 else (0, 1)[i - n + 2] for i in range(n)]
             flag = core
         else:
-            order = [((i // 2 + 1) // 2) % 2 for i in range(n)]
+            order = [((i + 1) // 2) % 2 for i in range(n)]
             flag = odd
         places = range(k * BATCH, (k + 1) * BATCH)
         even = [i for i in places if order[i] == 0]
         uneven = [i for i in places if order[i] == 1]
         flag = flag if mine else 1 - flag
-        where = arrival if l == 0 else by_owner
+        where = arrival if l == 0 else by_distance
         return [where(lax.select(flag == 0, e, u)) for e, u in zip(even, uneven, strict=True)]
 
     barrier = pltpu.get_barrier_semaphore()
@@ -172,12 +169,10 @@
 
     def send_rows(l):
         def far_first(k, carry):
-            t = by_distance(n // 2 - k)
-            row_copy(l, tp, t, send_sem.at[l, 0]).start()
-            row_copy(l, opposite, t, send_sem.at[l, 0]).start()
+            row_copy(l, tp, by_distance(n - k), send_sem.at[l, 0]).start()
             return carry
 
-        lax.fori_loop(1, n // 2, far_first, 0)
+        lax.fori_loop(1, n, far_first, 0, unroll=True)
 
     @pl.when(jnp.logical_not(at_hub))
     def _():
@@ -270,7 +265,7 @@
 
             lax.fori_loop(0, j + 1, catch_up, 0)
 
-            @pl.when(j > 0)
+            @pl.when((j > 0) & (j < n - 2))
             def _():
                 settle(j - 1)
 
@@ -283,6 +278,7 @@
 
         lax.fori_loop(0, n - 1, relay, 0)
         settle(n - 2)
+        settle(n - 3)
 
     loads[12].wait()
 
@@ -292,7 +288,7 @@
         def project(k):
             sources = batch_of(l, k)
             for t in sources:
-                @pl.when((t != tp) & (jnp.logical_not(at_hub) if l == 0 else t != opposite))
+                @pl.when((t != tp) & jnp.logical_not(at_hub) if l == 0 else t != tp)
                 def _(t=t):
                     wait_rows(l, t)
 
@@ -353,18 +349,31 @@
         if l == 0:
             for k in range(last):
                 project(k)
+            late = tp == n - 1
+
+            @pl.when(late)
+            def _():
+                project(last)
 
             @pl.when(jnp.logical_not(at_hub))
             def _():
                 with jax.named_scope("ready"):
                     pl.semaphore_wait(ready_sem, 1)
 
+            @pl.when(late)
+            def _():
+                give(last)
+
             for k in range(last):
                 give(k)
             for k in range(last):
                 pass_on(k)
-            project(last)
-            give(last)
+
+            @pl.when(jnp.logical_not(late))
+            def _():
+                project(last)
+                give(last)
+
         else:
             for k in range(last + 1):
                 project(k)
@@ -448,7 +457,7 @@
             return carry
 
         with jax.named_scope(f"send_m{l}"):
-            lax.fori_loop(1, n, send_mixed, 0)
+            lax.fori_loop(1, n, send_mixed, 0, unroll=True)
 
         nrm_o[l] = normalizer
         key_rows = stack(keys)
@@ -467,8 +476,6 @@
                         keep_h[h] * mem_t[l, r] + spread_key * value_h[h]
                     )
 
-        owners = 2 if l + 1 < layers else 1
-
         def leave(k, carry):
             homes = [by_distance(k * BATCH + j) for j in range(BATCH)]
             if l == 0:
@@ -490,49 +497,40 @@
                 osend[l, t] = part[j * rows : (j + 1) * rows].astype(BF16)
             for t in reversed(homes):
 
-                for owner in range(owners):
-                    home = lax.rem(t + owner * (n // 2), n)
-
-                    @pl.when(home == tp)
-                    def _(t=t, owner=owner):
-                        orecv[l, owner, tp] = osend[l, t]
-
-                    @pl.when(home != tp)
-                    def _(t=t, owner=owner, home=home):
-                        pltpu.make_async_remote_copy(
-                            src_ref=osend.at[l, t],
-                            dst_ref=orecv.at[l, owner, tp],
-                            send_sem=send_sem.at[l, 3 + 2 * owner],
-                            recv_sem=o_sem.at[l, owner],
-                            device_id={"tp": home},
-                            device_id_type=MESH,
-                        ).start()
+                @pl.when(t == tp)
+                def _(t=t):
+                    orecv[l, tp] = osend[l, t]
+
+                @pl.when(t != tp)
+                def _(t=t):
+                    pltpu.make_async_remote_copy(
+                        src_ref=osend.at[l, t],
+                        dst_ref=orecv.at[l, tp],
+                        send_sem=send_sem.at[l, 3],
+                        recv_sem=o_sem.at[l],
+                        device_id={"tp": t},
+                        device_id_type=MESH,
+                    ).start()
 
             return carry
 
         lax.fori_loop(0, n // BATCH, leave, 0)
 
-        for owner in range(owners):
-            some = orecv.at[l, owner, pl.ds(0, n - 1)]
-            with jax.named_scope(f"wait_o{l}"):
-                pltpu.make_async_copy(some, some, o_sem.at[l, owner]).wait()
-        for owner in range(owners):
-            home = (tp, opposite)[owner]
-            total = orecv[l, owner, 0].astype(F32)
-            for s in range(1, n):
-                total = total + orecv[l, owner, s].astype(F32)
-            rows_out = (xall[l, home].astype(F32) + total).astype(BF16)
-            if l + 1 < layers:
-                xall[l + 1, home] = rows_out
-            else:
-                tok_o[...] = rows_out
+        some = orecv.at[l, pl.ds(0, n - 1)]
+        with jax.named_scope(f"wait_o{l}"):
+            pltpu.make_async_copy(some, some, o_sem.at[l]).wait()
+        total = orecv[l, 0].astype(F32)
+        for s in range(1, n):
+            total = total + orecv[l, s].astype(F32)
+        rows_out = (xall[l, tp].astype(F32) + total).astype(BF16)
         if l + 1 < layers:
+            xall[l + 1, tp] = rows_out
             send_rows(l + 1)
+        else:
+            tok_o[...] = rows_out
 
     for l in range(layers):
-        sent = [(xall, n - 2), (psend, n // 2 - 1), (mixall, n - 1), (osend, n - 1), (pfull, n // 2)]
-        if l + 1 < layers:
-            sent.append((osend, n - 1))
+        sent = ((xall, n - 1), (psend, n // 2 - 1), (mixall, n - 1), (osend, n - 1), (pfull, n // 2))
         for k, (buffer, count) in enumerate(sent):
             some = buffer.at[l, pl.ds(0, count)]
             if l > 0 or k > 0:
@@ -630,14 +628,14 @@
             vmem((layers, n // 2, rows, block), BF16),
             vmem((layers, n, rows, width), BF16),
             vmem((layers, n, rows, width), BF16),
-            vmem((layers, 2, n, rows, width), BF16),
+            vmem((layers, n, rows, width), BF16),
             pltpu.SemaphoreType.DMA((13,)),
             pltpu.SemaphoreType.DMA((layers, n)),
             pltpu.SemaphoreType.DMA((layers, n)),
             pltpu.SemaphoreType.DMA((layers,)),
             pltpu.SemaphoreType.DMA((layers, n)),
-            pltpu.SemaphoreType.DMA((layers, 2)),
-            pltpu.SemaphoreType.DMA((layers, 6)),
+            pltpu.SemaphoreType.DMA((layers,)),
+            pltpu.SemaphoreType.DMA((layers, 5)),
             pltpu.SemaphoreType.DMA((n,)),
             pltpu.SemaphoreType.REGULAR((n,)),
             pltpu.SemaphoreType.REGULAR,

time: 104 us -> 103 us (level)
  no operation moved by 1% of the time
where the time goes in v4:
time: 103 us
  Pallas kernels  103 us (100%)
    pallas_call x1, Pallas kernels, per_device(): pl.pallas_call(functools.partial(kernel, n, layers), out_shape=(pltpu.VME...  102 us

profile of v4, /device:TPU:80, one launch (start us, length us, event | category | flops | bytes accessed | tf_op | source)
XLA Modules:
  0.0 103.3 jit_solution(16290802156553014321)
XLA Ops:
  0.6 101.6 %cells.1 = (bf16[8,256]{1,0:T(8,128)(2,1)S(1)}, f32[2,1024,128]{2,1,0:T(8,128)S(1)}, f32[2,8,256]{2,1,0:T(8,128)S(1)}, f32[2,4,8]{2,1,0:T(4,128)S(1)}) custom-call(bf16[8,256]{1,0:T(8,128)(2,1)} %tok_h.1, f32[2,256]{1,0:T(2,128)} %gain_h.1, bf16[2,256,256]{2,1,0:T(8,128)(2,1)} %qw_h.1, bf16[2,256,256]{2,1,0:T(8,128)(2,1)} %kw_h.1, ...), custom_call_target="tpu_custom_call" | custom-call | tf_op jit(solution)/shard_map/cells/pallas_call | solution.py:600
  102.3 1.1 %put_out.1 = (bf16[8,256]{1,0:T(8,128)(2,1)}, f32[2,1024,128]{2,1,0:T(8,128)}, f32[2,8,256]{2,1,0:T(8,128)}, f32[2,4,8]{2,1,0:T(4,128)}) custom-call(bf16[8,256]{1,0:T(8,128)(2,1)S(1)} %get-tuple-element.12.refs_0_, f32[2,1024,128]{2,1,0:T(8,128)S(1)} %get-tuple-element.13.refs_1_, f32[2,8,256]{2,1,0:T(8,128)S(1)} %get-tuple-element.14.refs_2_, ...), custom_call_target="tpu_custom_call" | custom-call | tf_op jit(solution)/shard_map/put_out/pallas_call | solution.py:668
